TPU v7x, 32 devices: a whole 2x2x4 slice. The times are simulated.
32 devices in a mesh: ep: 8 (over z, x), tp: 4 (over y, core).
Axes of the slice: x: 2, y: 2, z: 4, core: 2. Of those that a mesh axis runs over, the one named last changes fastest.
Arguments:
- tokens: bfloat16 [128, 1024], P('ep'), may hold values from -6 to 6
- memory: float32 [128, 4, 128, 256], P('ep', 'tp'), may hold values from -6 to 6
- log_scale: float32 [128, 4], P('ep', 'tp'), may hold values from -1 to 130
- mix_gain_in: float32 [1024], replicated, may hold values from 0.1 to 1.9
- w_query: bfloat16 [1024, 512], P(None, 'tp'), may hold values from -0.1875 to 0.1875
- w_key: bfloat16 [1024, 512], P(None, 'tp'), may hold values from -0.1875 to 0.1875
- w_value: bfloat16 [1024, 1024], P(None, 'tp'), may hold values from -0.1875 to 0.1875
- w_igate: bfloat16 [1024, 4], P(None, 'tp'), may hold values from -0.1875 to 0.1875
- w_fgate: bfloat16 [1024, 4], P(None, 'tp'), may hold values from -0.1875 to 0.1875
- igate_bias: float32 [4], P('tp'), may hold values from -1 to 1
- fgate_bias: float32 [4], P('tp'), may hold values from 0 to 4
- head_gain: float32 [1024], P('tp'), may hold values from 0.1 to 1.9
- w_output: bfloat16 [1024, 1024], P('tp'), may hold values from -0.1875 to 0.1875
- mix_gain_out: float32 [1024], replicated, may hold values from 0.1 to 1.9
- ffn_gain_in: float32 [1024], replicated, may hold values from 0.1 to 1.9
- routes: int32 [128, 6], P('ep'), may hold values from 0 to 7, all different within a row; in each aligned block of 16 rows (0 to 15, 16 to 31, ...) at most 16 rows name the same one
- route_weights: float32 [128, 6], P('ep'), may hold values from 0.1 to 1
- expert_gate: bfloat16 [8, 1024, 1024], P('ep', None, 'tp'), may hold values from -0.1875 to 0.1875
- expert_up: bfloat16 [8, 1024, 1024], P('ep', None, 'tp'), may hold values from -0.1875 to 0.1875
- expert_down: bfloat16 [8, 1024, 1024], P('ep', 'tp'), may hold values from -0.9375 to 0.9375
- ffn_gain_out: float32 [1024], P('tp'), may hold values from 0.1 to 1.9
Outputs:
- output: bfloat16 [128, 1024], P('ep', 'tp')
Inputs may be any that keep to these rules, and one draw needn't show every extreme that they name: `routes`: among the 16 tokens of one index of ep no expert is named by more than 16 tokens, and in every draw some expert is named by exactly 16 of them.
All inputs are finite; a program needn't handle non-finite values.
Results may differ from a plain program's by a relative error of at most 0.02.
Values may be sent and summed in bfloat16 or wider, within the bound.
A program may use at most 64 MiB of HBM per device.

v0:
```python
import functools

import jax
import jax.numpy as jnp
from jax import lax
from jax.experimental import pallas as pl
from jax.experimental.pallas import tpu as pltpu
from jax.sharding import PartitionSpec as P

EPS = 1e-06


def rms_scale(values):
    return lax.rsqrt(jnp.mean(values * values, axis=-1, keepdims=True) + EPS)


def routed_device(
    tokens,
    memory,
    log_scale,
    mix_gain_in,
    w_query,
    w_key,
    w_value,
    w_igate,
    w_fgate,
    igate_bias,
    fgate_bias,
    head_gain,
    w_output,
    mix_gain_out,
    ffn_gain_in,
    routes,
    route_weights,
    expert_gate,
    expert_up,
    expert_down,
    ffn_gain_out,
):
    f32 = jnp.float32
    bf16 = jnp.bfloat16
    seqs, width = tokens.shape
    heads = log_scale.shape[1]
    key_dim = memory.shape[2]
    value_dim = memory.shape[3]
    xf = tokens.astype(f32)
    normed = (xf * rms_scale(xf) * mix_gain_in).astype(bf16)
    query = jnp.dot(normed, w_query, preferred_element_type=f32).reshape(
        seqs, heads, key_dim
    ) * key_dim ** (-0.5)
    keys = jnp.dot(normed, w_key, preferred_element_type=f32).reshape(seqs, heads, key_dim)
    values = jnp.dot(normed, w_value, preferred_element_type=f32).reshape(seqs, heads, value_dim)
    in_pre = jnp.dot(normed, w_igate, preferred_element_type=f32) + igate_bias
    forget_log = jax.nn.log_sigmoid(
        jnp.dot(normed, w_fgate, preferred_element_type=f32) + fgate_bias
    )
    carried = forget_log + log_scale
    new_max = jnp.maximum(carried, in_pre)
    carry_weight = jnp.exp(carried - new_max)
    fresh_weight = jnp.exp(in_pre - new_max)
    recall = jnp.einsum("shk,shkv->shv", query, memory, precision=lax.Precision.HIGHEST)
    match = jnp.sum(query * keys, axis=-1)
    read = carry_weight[..., None] * recall + (fresh_weight * match)[..., None] * values
    headout = (
        (read * rms_scale(read) * head_gain.reshape(heads, value_dim))
        .astype(bf16)
        .reshape(seqs, heads * value_dim)
    )
    partial_value = jnp.dot(headout, w_output, preferred_element_type=f32)
    mixed = lax.psum(partial_value.astype(jnp.bfloat16), "tp").astype(jnp.float32)
    resid = (xf + mixed * rms_scale(mixed) * mix_gain_out).astype(bf16)
    rf = resid.astype(f32)
    ffn_in = (rf * rms_scale(rf) * ffn_gain_in).astype(bf16)
    lanes = lax.axis_size("tp")
    quarter = width // lanes
    own = lax.axis_index("tp") * quarter
    local_experts = expert_gate.shape[0]
    experts_all = local_experts * lax.axis_size("ep")
    top = routes.shape[1]
    cap = min(seqs, max(2, 3 * seqs * top // (2 * experts_all)))
    flat = routes.reshape(-1)
    hits = (flat[:, None] == jnp.arange(experts_all, dtype=jnp.int32)[None, :]).astype(jnp.int32)
    earlier = jnp.cumsum(hits, axis=0) - hits
    slot = jnp.sum(earlier * hits, axis=1)
    place = (flat * cap + slot).reshape(seqs, top)
    picker = jnp.any(
        jnp.arange(experts_all * cap, dtype=jnp.int32)[:, None, None] == place[None, :, :], axis=2
    ).astype(bf16)
    outbound = (
        jnp.dot(picker, ffn_in, preferred_element_type=f32)
        .astype(bf16)
        .reshape(experts_all, cap, width)
    )
    arrived = lax.all_to_all(outbound, "ep", split_axis=0, concat_axis=0, tiled=True)
    items = arrived.shape[1]
    rows = arrived.reshape(-1, local_experts, items, width)
    gate = jnp.einsum("secd,edf->secf", rows, expert_gate, preferred_element_type=f32)
    up = jnp.einsum("secd,edf->secf", rows, expert_up, preferred_element_type=f32)
    act = (jax.nn.silu(gate) * up).astype(bf16)
    part = jnp.einsum("secf,efd->secd", act, expert_down, preferred_element_type=f32).reshape(
        -1, items, width
    )
    summed = lax.psum_scatter(
        part.astype(jnp.bfloat16), "tp", scatter_dimension=2, tiled=True
    ).astype(jnp.float32)
    done = summed.astype(bf16)
    returned = lax.all_to_all(done, "ep", split_axis=0, concat_axis=0, tiled=True)
    columns = returned.shape[2]
    chosen = jnp.take(returned.reshape(-1, columns), place.reshape(-1), axis=0).reshape(
        seqs, top, columns
    )
    routed = jnp.sum(route_weights[:, :, None] * chosen.astype(f32), axis=1)
    resid_part = lax.dynamic_slice_in_dim(rf, own, quarter, 1)
    total = lax.psum(jnp.sum(routed * routed, axis=1), "tp")
    scaled = routed * lax.rsqrt(total / width + EPS)[:, None]
    return (resid_part + scaled * ffn_gain_out).astype(bf16)


F32 = jnp.float32
BF16 = jnp.bfloat16
MESH = pl.DeviceIdType.MESH


def column_of(row):
    n = row.shape[1]
    eye = lax.broadcasted_iota(jnp.int32, (n, n), 0) == lax.broadcasted_iota(jnp.int32, (n, n), 1)
    return jnp.sum(jnp.where(eye, jnp.broadcast_to(row, (n, n)), 0.0), axis=1, keepdims=True)


def layer_kernel(
    groups,
    lanes,
    tokens_hbm,
    memory_hbm,
    log_scale_hbm,
    gain_in_hbm,
    w_query_hbm,
    w_key_hbm,
    w_value_hbm,
    w_igate_hbm,
    w_fgate_hbm,
    igate_bias_ref,
    fgate_bias_ref,
    head_gain_hbm,
    w_output_hbm,
    gain_out_hbm,
    ffn_gain_hbm,
    routes_hbm,
    route_weights_hbm,
    gate_hbm,
    up_hbm,
    down_hbm,
    ffn_gain_out_hbm,
    out_ref,
    log_scale_ref,
    gain_in_ref,
    w_igate_ref,
    w_fgate_ref,
    head_gain_ref,
    gain_out_ref,
    ffn_gain_ref,
    routes_ref,
    route_weights_ref,
    ffn_gain_out_ref,
    small_sem,
    tokens_v,
    memory_v,
    w_query_v,
    w_key_v,
    w_value_v,
    w_output_v,
    gate_v,
    up_v,
    down_v,
    recall_v,
    shares,
    rows,
    inbox,
    resid_v,
    parts,
    results,
    squares,
    load_sem,
    memory_sem,
    pair_send,
    pair_recv,
    share_send,
    share_recv,
    rows_send,
    rows_recv,
    parts_send,
    parts_recv,
    squares_send,
    squares_recv,
):
    ep = lax.axis_index("ep")
    tp = lax.axis_index("tp")
    seqs, width = tokens_v.shape
    key_dim = memory_v.shape[1]
    value_dim = memory_v.shape[2]
    quarter = width // lanes
    core, chip = lax.rem(tp, 2), tp // 2
    slots, chips, half = groups // 2, lanes // 2, width // 2

    def device(off, toff):
        return (lax.rem(ep + (off % groups), groups), lax.rem(tp + (toff % lanes), lanes))

    barrier = pltpu.get_barrier_semaphore()
    for off in range(groups):
        for toff in range(lanes):
            if off or toff:
                pl.semaphore_signal(
                    barrier, inc=1, device_id=device(off, toff), device_id_type=MESH
                )

    def partner(off):
        index, bit = 0, 1
        while bit < groups:
            index += bit * lax.rem(ep // bit + off // bit, 2)
            bit *= 2
        return index

    pieces = memory_sem.shape[0]
    piece = seqs // pieces
    loads = {}
    for i, (name, src, dst) in enumerate(
        (
            ("tokens", tokens_hbm, tokens_v),
            ("query", w_query_hbm, w_query_v),
            ("key", w_key_hbm, w_key_v),
            ("value", w_value_hbm, w_value_v),
            ("output", w_output_hbm, w_output_v),
            ("gate", gate_hbm.at[0], gate_v.at[0]),
            ("up", up_hbm.at[0], up_v.at[0]),
            ("down", down_hbm.at[0], down_v.at[0]),
        )
    ):
        loads[name] = pltpu.make_async_copy(src, dst, load_sem.at[i])
    memory_loads = [
        pltpu.make_async_copy(
            memory_hbm.at[pl.ds(i * piece, piece), 0],
            memory_v.at[pl.ds(i * piece, piece)],
            memory_sem.at[i],
        )
        for i in range(pieces)
    ]
    small = [
        pltpu.make_async_copy(src, dst, small_sem.at[i])
        for i, (src, dst) in enumerate(
            (
                (log_scale_hbm, log_scale_ref),
                (gain_in_hbm, gain_in_ref),
                (w_igate_hbm, w_igate_ref),
                (w_fgate_hbm, w_fgate_ref),
                (head_gain_hbm, head_gain_ref),
                (gain_out_hbm, gain_out_ref),
                (ffn_gain_hbm, ffn_gain_ref),
                (routes_hbm, routes_ref),
                (route_weights_hbm, route_weights_ref),
                (ffn_gain_out_hbm, ffn_gain_out_ref),
            )
        )
    ]
    loads["tokens"].start()
    for load in small:
        load.start()
    for name in ("query", "key", "value"):
        loads[name].start()
    for load in memory_loads:
        load.start()
    for name in ("output", "gate", "up", "down"):
        loads[name].start()

    loads["tokens"].wait()
    for load in small:
        load.wait()
    xf = tokens_v[...].astype(F32)
    normed = (xf * rms_scale(xf) * gain_in_ref[...]).astype(BF16)
    nf = normed.astype(F32)
    in_pre = (
        jnp.sum(nf * w_igate_ref[...].astype(F32), axis=1, keepdims=True) + igate_bias_ref[0]
    )
    fpre = jnp.sum(nf * w_fgate_ref[...].astype(F32), axis=1, keepdims=True) + fgate_bias_ref[0]
    forget_log = jnp.minimum(fpre, 0.0) - jnp.log1p(jnp.exp(-jnp.abs(fpre)))
    carried = forget_log + column_of(log_scale_ref[...])
    new_max = jnp.maximum(carried, in_pre)
    carry_weight = jnp.exp(carried - new_max)
    fresh_weight = jnp.exp(in_pre - new_max)
    loads["query"].wait()
    query = jnp.dot(normed, w_query_v[...], preferred_element_type=F32) * key_dim ** (-0.5)
    loads["key"].wait()
    keys = jnp.dot(normed, w_key_v[...], preferred_element_type=F32)
    loads["value"].wait()
    values = jnp.dot(normed, w_value_v[...], preferred_element_type=F32)
    match = jnp.sum(query * keys, axis=1, keepdims=True)
    turned = query.T
    for i in range(pieces):
        memory_loads[i].wait()
        for s in range(i * piece, (i + 1) * piece):
            recall_v[s : s + 1, :] = jnp.sum(
                turned[:, s : s + 1] * memory_v[s], axis=0, keepdims=True
            )
    read = carry_weight * recall_v[...] + (fresh_weight * match) * values
    headout = (read * rms_scale(read) * head_gain_ref[...]).astype(BF16)
    loads["output"].wait()
    shares[0] = jnp.dot(headout, w_output_v[...], preferred_element_type=F32).astype(BF16)

    pl.semaphore_wait(barrier, groups * lanes - 1)
    copies = []
    for toff in range(1, lanes):
        copy = pltpu.make_async_remote_copy(
            src_ref=shares.at[0],
            dst_ref=shares.at[toff],
            send_sem=share_send.at[toff],
            recv_sem=share_recv.at[toff],
            device_id=device(0, toff),
            device_id_type=MESH,
        )
        copy.start()
        copies.append(copy)
    pairs = []
    for i, (name, ref) in enumerate((("gate", gate_v), ("up", up_v), ("down", down_v))):
        loads[name].wait()
        copy = pltpu.make_async_remote_copy(
            src_ref=ref.at[0],
            dst_ref=ref.at[1],
            send_sem=pair_send.at[i],
            recv_sem=pair_recv.at[i],
            device_id=(ep, tp + 1 - 2 * core),
            device_id_type=MESH,
        )
        copy.start()
        pairs.append(copy)
    mine = [
        column_of(
            jnp.sum(
                jnp.where(
                    routes_ref[...] == partner(off), route_weights_ref[...], 0.0
                ),
                axis=0,
                keepdims=True,
            )
        )
        for off in range(groups)
    ]
    mixed = shares[0].astype(F32)
    for toff in range(1, lanes):
        copies[toff - 1].wait_recv()
        mixed = mixed + shares[toff].astype(F32)
    resid = (xf + mixed * rms_scale(mixed) * gain_out_ref[...]).astype(BF16)
    rf = resid.astype(F32)
    ffn_in = (rf * rms_scale(rf) * ffn_gain_ref[...]).astype(BF16)
    for h in range(2):
        rows[h] = ffn_in[:, h * half : (h + 1) * half]
    for off in range(1, groups):
        copy = pltpu.make_async_remote_copy(
            src_ref=rows.at[core],
            dst_ref=inbox.at[core, off // 2],
            send_sem=rows_send.at[off],
            recv_sem=rows_recv.at[core, off // 2],
            device_id=(partner(off), 2 * chip + off % 2),
            device_id_type=MESH,
        )
        copy.start()
        copies.append(copy)
    for q in range(lanes):
        resid_v[q] = rf[:, q * quarter : (q + 1) * quarter]

    def arrived(ref, sem):
        pltpu.make_async_copy(ref, ref, sem).wait()

    @pl.when(core == 0)
    def _():
        for h in range(2):
            inbox[h, 0] = ffn_in[:, h * half : (h + 1) * half]

    @pl.when(core == 1)
    def _():
        for h in range(2):
            arrived(inbox.at[h, 0], rows_recv.at[h, 0])

    for copy in pairs:
        copy.wait_recv()

    def result(slot, toff):
        group = partner(2 * slot) + core * (1 - 2 * lax.rem(ep, 2))
        return pltpu.make_async_remote_copy(
            src_ref=parts.at[lax.rem(tp + toff, lanes), slot],
            dst_ref=results.at[2 * slot + core, chip],
            send_sem=parts_send.at[slot, toff],
            recv_sem=parts_recv.at[2 * slot + core, chip],
            device_id=(group, lax.rem(tp + toff, lanes)),
            device_id_type=MESH,
        )

    for first, count in ((slot, 1) for slot in range(slots)):
        for slot in range(max(first, 1), first + count):
            for h in range(2):
                arrived(inbox.at[h, slot], rows_recv.at[h, slot])
        x = [inbox[h, first : first + count].reshape(count * seqs, half) for h in range(2)]

        def into(weights, block):
            return sum(
                jnp.dot(
                    x[h], weights[block, h * half : (h + 1) * half, :], preferred_element_type=F32
                )
                for h in range(2)
            )

        act = [
            (jax.nn.silu(into(gate_v, block)) * into(up_v, block)).astype(BF16)
            for block in range(2)
        ]
        for q in range(lanes):
            parts[q, first : first + count] = (
                sum(
                    jnp.dot(
                        act[block],
                        down_v[block, :, q * quarter : (q + 1) * quarter],
                        preferred_element_type=F32,
                    )
                    for block in range(2)
                )
                .astype(BF16)
                .reshape(count, seqs, quarter)
            )
        for slot in range(first, first + count):
            for toff in range(lanes - 1, -1, -1):
                if slot or toff:
                    result(slot, toff).start()
        if first == 0:

            @pl.when(core == 1)
            def _():
                result(0, 0).start()

            @pl.when(core == 0)
            def _():
                results[0, chip] = parts[tp, 0]

    routed = None
    for off in range(groups):
        total = None
        for y in range(chips):
            if off:
                arrived(results.at[off, y], parts_recv.at[off, y])
            else:

                @pl.when((core == 1) | (chip != y))
                def _():
                    arrived(results.at[off, y], parts_recv.at[off, y])

            part = results[off, y].astype(F32)
            total = part if total is None else total + part
        term = mine[off] * total.astype(BF16).astype(F32)
        routed = term if routed is None else routed + term
    wide = squares.shape[2]
    eye = lax.broadcasted_iota(jnp.int32, (seqs, wide), 0) == lax.broadcasted_iota(
        jnp.int32, (seqs, wide), 1
    )
    squares[0] = jnp.sum(
        jnp.where(eye, jnp.sum(routed * routed, axis=1, keepdims=True), 0.0),
        axis=0,
        keepdims=True,
    )
    last = []
    for toff in range(1, lanes):
        copy = pltpu.make_async_remote_copy(
            src_ref=squares.at[0],
            dst_ref=squares.at[toff],
            send_sem=squares_send.at[toff],
            recv_sem=squares_recv.at[toff],
            device_id=device(0, toff),
            device_id_type=MESH,
        )
        copy.start()
        last.append(copy)
    for copy in copies:
        copy.wait_send()
    for copy in pairs:
        copy.wait_send()
    for slot in range(slots):
        for toff in range(lanes):
            if slot or toff:
                result(slot, toff).wait_send()

    @pl.when(core == 1)
    def _():
        result(0, 0).wait_send()

    total = squares[0]
    for toff in range(1, lanes):
        last[toff - 1].wait_recv()
        total = total + squares[toff]
    scale = jnp.sum(
        jnp.where(eye, lax.rsqrt(total / width + EPS), 0.0), axis=1, keepdims=True
    )
    scaled = routed * scale
    out_ref[...] = (resid_v[tp] + scaled * ffn_gain_out_ref[...]).astype(BF16)
    for copy in last:
        copy.wait_send()


def per_device(*args):
    (
        tokens,
        memory,
        log_scale,
        mix_gain_in,
        w_query,
        w_key,
        w_value,
        w_igate,
        w_fgate,
        igate_bias,
        fgate_bias,
        head_gain,
        w_output,
        mix_gain_out,
        ffn_gain_in,
        routes,
        route_weights,
        expert_gate,
        expert_up,
        expert_down,
        ffn_gain_out,
    ) = args
    groups = lax.axis_size("ep")
    lanes = lax.axis_size("tp")
    seqs, width = tokens.shape
    local_experts, _, hidden = expert_gate.shape
    top = routes.shape[1]
    if local_experts != 1 or log_scale.shape[1] != 1 or 2 * top < groups or groups & (groups - 1) or groups < 4 or lanes % 2:
        return routed_device(*args)
    quarter = width // lanes
    key_dim, value_dim = memory.shape[2:]
    vmem = pl.BlockSpec(memory_space=pltpu.VMEM)
    hbm = pl.BlockSpec(memory_space=pl.ANY)
    smem = pl.BlockSpec(memory_space=pltpu.SMEM)
    dma = pltpu.SemaphoreType.DMA
    pieces = 4 if seqs % 4 == 0 else 1
    operands = (
        (tokens, hbm),
        (memory, hbm),
        (log_scale.T, hbm),
        (mix_gain_in.reshape(1, -1), hbm),
        (w_query, hbm),
        (w_key, hbm),
        (w_value, hbm),
        (w_igate.T, hbm),
        (w_fgate.T, hbm),
        (igate_bias, smem),
        (fgate_bias, smem),
        (head_gain.reshape(1, -1), hbm),
        (w_output, hbm),
        (mix_gain_out.reshape(1, -1), hbm),
        (ffn_gain_in.reshape(1, -1), hbm),
        (routes.T, hbm),
        (route_weights.T, hbm),
        (expert_gate, hbm),
        (expert_up, hbm),
        (expert_down, hbm),
        (ffn_gain_out.reshape(1, -1), hbm),
    )
    return pl.pallas_call(
        functools.partial(layer_kernel, groups, lanes),
        out_shape=pltpu.VMEM((seqs, quarter), BF16),
        in_specs=[spec for _, spec in operands],
        out_specs=vmem,
        scratch_shapes=[
            *[pltpu.VMEM(operands[i][0].shape, operands[i][0].dtype) for i in (2, 3, 7, 8, 11, 13, 14, 15, 16, 20)],
            dma((10,)),
            pltpu.VMEM((seqs, width), BF16),
            pltpu.VMEM((seqs, key_dim, value_dim), F32),
            pltpu.VMEM(w_query.shape, BF16),
            pltpu.VMEM(w_key.shape, BF16),
            pltpu.VMEM(w_value.shape, BF16),
            pltpu.VMEM(w_output.shape, BF16),
            pltpu.VMEM((2, width, hidden), BF16),
            pltpu.VMEM((2, width, hidden), BF16),
            pltpu.VMEM((2, hidden, width), BF16),
            pltpu.VMEM((seqs, value_dim), F32),
            pltpu.VMEM((lanes, seqs, width), BF16),
            pltpu.VMEM((2, seqs, width // 2), BF16),
            pltpu.VMEM((2, groups // 2, seqs, width // 2), BF16),
            pltpu.VMEM((lanes, seqs, quarter), F32),
            pltpu.VMEM((lanes, groups // 2, seqs, quarter), BF16),
            pltpu.VMEM((groups, lanes // 2, seqs, quarter), BF16),
            pltpu.VMEM((lanes, 1, 128), F32),
            dma((8,)),
            dma((pieces,)),
            dma((3,)),
            dma((3,)),
            dma((lanes,)),
            dma((lanes,)),
            dma((groups,)),
            dma((2, groups // 2)),
            dma((groups // 2, lanes)),
            dma((groups, lanes // 2)),
            dma((lanes,)),
            dma((lanes,)),
        ],
        compiler_params=pltpu.CompilerParams(
            collective_id=0,
            has_side_effects=True,
            vmem_limit_bytes=59 * 1024 * 1024,
        ),
        name="layer",
    )(*[array for array, _ in operands])


def solution(mesh):
    return jax.shard_map(
        per_device,
        mesh=mesh,
        in_specs=(
            P("ep", None),
            P("ep", "tp", None, None),
            P("ep", "tp"),
            P(),
            P(None, "tp"),
            P(None, "tp"),
            P(None, "tp"),
            P(None, "tp"),
            P(None, "tp"),
            P("tp"),
            P("tp"),
            P("tp"),
            P("tp", None),
            P(),
            P(),
            P("ep", None),
            P("ep", None),
            P("ep", None, "tp"),
            P("ep", None, "tp"),
            P("ep", "tp", None),
            P("tp"),
        ),
        out_specs=P("ep", "tp"),
        check_vma=False,
    )
```

profile of v0, /device:TPU:0, one launch (start us, length us, event | category | flops | bytes accessed | tf_op | source)
XLA Modules:
  0.0 26.1 jit_solution(5715038395065990005)
XLA Ops:
  1.3 24.2 %layer.1 = bf16[16,256]{1,0:T(8,128)(2,1)S(1)} custom-call(bf16[16,1024]{1,0:T(8,128)(2,1)} %tokens_hbm.1, f32[16,1,128,256]{3,2,1,0:T(8,128)} %memory_hbm.1, f32[1,16]{1,0:T(1,128)} %bitcast.19, f32[1,1024]{1,0:T(1,128)} %bitcast.10, bf16[1024,128]{1,0:T(8,128)(2,1)} %w_query_hbm.1, bf16[1024,128]{1,0:T(8,128)(2,1)} %w_key_hbm.1, ...), custom_call_target="tpu_custom_call" | custom-call | tf_op jit(solution)/shard_map/layer/pallas_call | solution.py:565
  25.5 0.6 %copy.23 = bf16[16,256]{1,0:T(8,128)(2,1)} copy(bf16[16,256]{1,0:T(8,128)(2,1)S(1)} %layer.1) | data formatting | bytes 16384
where the time goes:
time: 26.3 us; the launch traced here: 26.1 us
  Pallas kernels  24.2 us (92%)
  between operations  1.3 us (5%)
  local copies, waits for them, and re-layouts  0.6 us (2%)
    pallas_call x1, Pallas kernels, per_device(): pl.pallas_call(functools.partial(layer_kernel, groups, lanes), out_shape=...  24.2 us
    unnamed x1, local copies, waits for them, and re-layouts  0.6 us

commit v1 on v0

v1 whole, which is shorter than its diff:
```python
import functools

import jax
import jax.numpy as jnp
from jax import lax
from jax.experimental import pallas as pl
from jax.experimental.pallas import tpu as pltpu
from jax.sharding import PartitionSpec as P

EPS = 1e-06


def rms_scale(values):
    return lax.rsqrt(jnp.mean(values * values, axis=-1, keepdims=True) + EPS)


def routed_device(
    tokens,
    memory,
    log_scale,
    mix_gain_in,
    w_query,
    w_key,
    w_value,
    w_igate,
    w_fgate,
    igate_bias,
    fgate_bias,
    head_gain,
    w_output,
    mix_gain_out,
    ffn_gain_in,
    routes,
    route_weights,
    expert_gate,
    expert_up,
    expert_down,
    ffn_gain_out,
):
    f32 = jnp.float32
    bf16 = jnp.bfloat16
    seqs, width = tokens.shape
    heads = log_scale.shape[1]
    key_dim = memory.shape[2]
    value_dim = memory.shape[3]
    xf = tokens.astype(f32)
    normed = (xf * rms_scale(xf) * mix_gain_in).astype(bf16)
    query = jnp.dot(normed, w_query, preferred_element_type=f32).reshape(
        seqs, heads, key_dim
    ) * key_dim ** (-0.5)
    keys = jnp.dot(normed, w_key, preferred_element_type=f32).reshape(seqs, heads, key_dim)
    values = jnp.dot(normed, w_value, preferred_element_type=f32).reshape(seqs, heads, value_dim)
    in_pre = jnp.dot(normed, w_igate, preferred_element_type=f32) + igate_bias
    forget_log = jax.nn.log_sigmoid(
        jnp.dot(normed, w_fgate, preferred_element_type=f32) + fgate_bias
    )
    carried = forget_log + log_scale
    new_max = jnp.maximum(carried, in_pre)
    carry_weight = jnp.exp(carried - new_max)
    fresh_weight = jnp.exp(in_pre - new_max)
    recall = jnp.einsum("shk,shkv->shv", query, memory, precision=lax.Precision.HIGHEST)
    match = jnp.sum(query * keys, axis=-1)
    read = carry_weight[..., None] * recall + (fresh_weight * match)[..., None] * values
    headout = (
        (read * rms_scale(read) * head_gain.reshape(heads, value_dim))
        .astype(bf16)
        .reshape(seqs, heads * value_dim)
    )
    partial_value = jnp.dot(headout, w_output, preferred_element_type=f32)
    mixed = lax.psum(partial_value.astype(jnp.bfloat16), "tp").astype(jnp.float32)
    resid = (xf + mixed * rms_scale(mixed) * mix_gain_out).astype(bf16)
    rf = resid.astype(f32)
    ffn_in = (rf * rms_scale(rf) * ffn_gain_in).astype(bf16)
    lanes = lax.axis_size("tp")
    quarter = width // lanes
    own = lax.axis_index("tp") * quarter
    local_experts = expert_gate.shape[0]
    experts_all = local_experts * lax.axis_size("ep")
    top = routes.shape[1]
    cap = min(seqs, max(2, 3 * seqs * top // (2 * experts_all)))
    flat = routes.reshape(-1)
    hits = (flat[:, None] == jnp.arange(experts_all, dtype=jnp.int32)[None, :]).astype(jnp.int32)
    earlier = jnp.cumsum(hits, axis=0) - hits
    slot = jnp.sum(earlier * hits, axis=1)
    place = (flat * cap + slot).reshape(seqs, top)
    picker = jnp.any(
        jnp.arange(experts_all * cap, dtype=jnp.int32)[:, None, None] == place[None, :, :], axis=2
    ).astype(bf16)
    outbound = (
        jnp.dot(picker, ffn_in, preferred_element_type=f32)
        .astype(bf16)
        .reshape(experts_all, cap, width)
    )
    arrived = lax.all_to_all(outbound, "ep", split_axis=0, concat_axis=0, tiled=True)
    items = arrived.shape[1]
    rows = arrived.reshape(-1, local_experts, items, width)
    gate = jnp.einsum("secd,edf->secf", rows, expert_gate, preferred_element_type=f32)
    up = jnp.einsum("secd,edf->secf", rows, expert_up, preferred_element_type=f32)
    act = (jax.nn.silu(gate) * up).astype(bf16)
    part = jnp.einsum("secf,efd->secd", act, expert_down, preferred_element_type=f32).reshape(
        -1, items, width
    )
    summed = lax.psum_scatter(
        part.astype(jnp.bfloat16), "tp", scatter_dimension=2, tiled=True
    ).astype(jnp.float32)
    done = summed.astype(bf16)
    returned = lax.all_to_all(done, "ep", split_axis=0, concat_axis=0, tiled=True)
    columns = returned.shape[2]
    chosen = jnp.take(returned.reshape(-1, columns), place.reshape(-1), axis=0).reshape(
        seqs, top, columns
    )
    routed = jnp.sum(route_weights[:, :, None] * chosen.astype(f32), axis=1)
    resid_part = lax.dynamic_slice_in_dim(rf, own, quarter, 1)
    total = lax.psum(jnp.sum(routed * routed, axis=1), "tp")
    scaled = routed * lax.rsqrt(total / width + EPS)[:, None]
    return (resid_part + scaled * ffn_gain_out).astype(bf16)


F32 = jnp.float32
BF16 = jnp.bfloat16
MESH = pl.DeviceIdType.MESH


def column_of(row):
    n = row.shape[1]
    eye = lax.broadcasted_iota(jnp.int32, (n, n), 0) == lax.broadcasted_iota(jnp.int32, (n, n), 1)
    return jnp.sum(jnp.where(eye, jnp.broadcast_to(row, (n, n)), 0.0), axis=1, keepdims=True)


def xor(a, b, size):
    total, bit = 0, 1
    while bit < size:
        total += bit * lax.rem(a // bit + b // bit, 2)
        bit *= 2
    return total


def arrived(ref, sem):
    pltpu.make_async_copy(ref, ref, sem).wait()


def layer_kernel(
    groups,
    lanes,
    tokens_hbm,
    memory_hbm,
    log_scale_hbm,
    gain_in_hbm,
    w_query_hbm,
    w_key_hbm,
    w_value_hbm,
    w_igate_hbm,
    w_fgate_hbm,
    igate_bias_hbm,
    fgate_bias_hbm,
    head_gain_hbm,
    w_output_hbm,
    gain_out_hbm,
    ffn_gain_hbm,
    routes_hbm,
    route_weights_hbm,
    gate_hbm,
    up_hbm,
    down_hbm,
    ffn_gain_out_hbm,
    out_ref,
    log_scale_ref,
    gain_in_ref,
    w_igate_ref,
    w_fgate_ref,
    igate_bias_ref,
    fgate_bias_ref,
    head_gain_ref,
    gain_out_ref,
    ffn_gain_ref,
    routes_ref,
    route_weights_ref,
    ffn_gain_out_ref,
    tokens_v,
    memory_v,
    w_qkv_v,
    w_output_v,
    gate_v,
    up_v,
    down_v,
    spread_v,
    recall_v,
    shares,
    rows,
    inbox,
    resid_v,
    parts,
    results,
    squares,
    load_sem,
    early_sem,
    late_sem,
    memory_sem,
    expert_sem,
    pair_send,
    pair_recv,
    entered,
    share_send,
    share_recv,
    rows_send,
    rows_recv,
    parts_send,
    parts_recv,
    squares_send,
    squares_recv,
):
    ep = lax.axis_index("ep")
    tp = lax.axis_index("tp")
    seqs, width = tokens_v.shape
    key_dim = memory_v.shape[1]
    value_dim = memory_v.shape[2]
    quarter = width // lanes
    core, chip = lax.rem(tp, 2), tp // 2
    slots, chips = groups // 2, lanes // 2
    depth, side = ep // 2, lax.rem(ep, 2)
    barrier = pltpu.get_barrier_semaphore()

    def lane_at(ahead, to_core):
        return 2 * lax.rem(chip + ahead, chips) + to_core

    pieces = memory_sem.shape[0]
    piece = seqs // pieces
    load_tokens = pltpu.make_async_copy(tokens_hbm, tokens_v, load_sem.at[0])
    load_gain = pltpu.make_async_copy(gain_in_hbm, gain_in_ref, load_sem.at[1])
    load_qkv = [
        pltpu.make_async_copy(src, w_qkv_v.at[:, pl.ds(at, src.shape[1])], load_sem.at[2])
        for src, at in (
            (w_query_hbm, 0),
            (w_key_hbm, key_dim),
            (w_value_hbm, 2 * key_dim),
        )
    ]
    load_output = pltpu.make_async_copy(w_output_hbm, w_output_v, load_sem.at[3])
    load_memory = [
        pltpu.make_async_copy(
            memory_hbm.at[pl.ds(i * piece, piece), 0],
            memory_v.at[pl.ds(i * piece, piece)],
            memory_sem.at[i],
        )
        for i in range(pieces)
    ]
    early = [
        pltpu.make_async_copy(src, dst, early_sem.at[i])
        for i, (src, dst) in enumerate(
            (
                (log_scale_hbm, log_scale_ref),
                (w_igate_hbm, w_igate_ref),
                (w_fgate_hbm, w_fgate_ref),
                (igate_bias_hbm, igate_bias_ref),
                (fgate_bias_hbm, fgate_bias_ref),
                (head_gain_hbm, head_gain_ref),
            )
        )
    ]
    late = [
        pltpu.make_async_copy(src, dst, late_sem.at[i])
        for i, (src, dst) in enumerate(
            (
                (gain_out_hbm, gain_out_ref),
                (ffn_gain_hbm, ffn_gain_ref),
                (routes_hbm, routes_ref),
                (route_weights_hbm, route_weights_ref),
                (ffn_gain_out_hbm, ffn_gain_out_ref),
            )
        )
    ]
    load_experts = [
        pltpu.make_async_copy(src.at[0], dst.at[0], expert_sem.at[i])
        for i, (src, dst) in enumerate(((gate_hbm, gate_v), (up_hbm, up_v), (down_hbm, down_v)))
    ]
    load_tokens.start()
    load_gain.start()
    for load in load_qkv:
        load.start()
    for load in load_memory:
        load.start()
    for load in early:
        load.start()
    load_output.start()

    def depth_of(slot):
        return slot - 1 + (slot - 1 + slots - depth) // slots

    def slot_of(group):
        return depth + (group // 2 - depth + slots - 1) // slots

    def greet(group, lane):
        pl.semaphore_signal(barrier, inc=1, device_id=(group, lane), device_id_type=MESH)

    for ahead in range(1, chips):
        greet(ep, lane_at(ahead, 0))
    for slot in range(1, slots):
        greet(xor(ep, 2 * slot + core, groups), 2 * chip + 1)

    @pl.when(core == 1)
    def _():
        greet(ep, tp - 1)
        greet(xor(ep, 1, groups), tp)

    for load in late:
        load.start()
    count = spread_v.shape[0]
    spread_v[...] = (
        lax.rem(lax.broadcasted_iota(jnp.int32, spread_v.shape, 0), seqs)
        == lax.broadcasted_iota(jnp.int32, spread_v.shape, 1) // key_dim
    ).astype(F32).astype(BF16)

    load_tokens.wait()
    load_gain.wait()
    xf = tokens_v[...].astype(F32)
    normed = (xf * rms_scale(xf) * gain_in_ref[...]).astype(BF16)
    arrived(w_qkv_v, load_sem.at[2])
    qkv = jnp.dot(normed, w_qkv_v[...], preferred_element_type=F32)
    query = qkv[:, :key_dim] * key_dim ** (-0.5)
    keys = qkv[:, key_dim : 2 * key_dim]
    values = qkv[:, 2 * key_dim :]
    for load in load_experts:
        load.start()
    for load in early:
        load.wait()
    nf = normed.astype(F32)
    in_pre = (
        jnp.sum(nf * w_igate_ref[...].astype(F32), axis=1, keepdims=True) + igate_bias_ref[...]
    )
    fpre = jnp.sum(nf * w_fgate_ref[...].astype(F32), axis=1, keepdims=True) + fgate_bias_ref[...]
    forget_log = jnp.minimum(fpre, 0.0) - jnp.log1p(jnp.exp(-jnp.abs(fpre)))
    carried = forget_log + column_of(log_scale_ref[...])
    new_max = jnp.maximum(carried, in_pre)
    carry_weight = jnp.exp(carried - new_max)
    fresh_weight = jnp.exp(in_pre - new_max)
    match = jnp.sum(query * keys, axis=1, keepdims=True)
    high = query.astype(BF16).astype(F32)
    middle = (query - high).astype(BF16).astype(F32)
    low = query - high - middle
    turned = jnp.concatenate([high, middle, low], axis=0).T.astype(BF16)

    @pl.when(core == 0)
    def _():
        pl.semaphore_wait(barrier, lanes - 1)
        pl.semaphore_signal(entered, inc=1, device_id=(ep, tp + 1), device_id_type=MESH)

    for i in range(pieces):
        load_memory[i].wait()
        wide = jnp.dot(
            turned,
            spread_v[:, i * piece * key_dim : (i + 1) * piece * key_dim],
            preferred_element_type=F32,
        )
        for j in range(piece):
            s = i * piece + j
            column = wide[:, j * key_dim : (j + 1) * key_dim]
            for at in range(0, value_dim, key_dim):
                recall_v[s : s + 1, at : at + key_dim] = jnp.sum(
                    column * memory_v[s, :, at : at + key_dim], axis=0, keepdims=True
                )
    read = carry_weight * recall_v[...] + (fresh_weight * match) * values
    headout = (read * rms_scale(read) * head_gain_ref[...]).astype(BF16)
    load_output.wait()
    shares[0] = jnp.dot(headout, w_output_v[...], preferred_element_type=F32).astype(BF16)

    @pl.when(core == 1)
    def _():
        pl.semaphore_wait(entered, 1)


    def share(ahead, to_core):
        pltpu.make_async_remote_copy(
            src_ref=shares.at[0],
            dst_ref=shares.at[2 * ahead + lax.rem(core + to_core, 2)],
            send_sem=share_send,
            recv_sem=share_recv,
            device_id=(ep, lane_at(ahead, to_core)),
            device_id_type=MESH,
        ).start()

    for ahead in range(1, chips):
        share(ahead, 1)
    share(0, 1 - core)
    for ahead in range(1, chips):
        share(ahead, 0)
    pairs = []
    for i, ref in enumerate((gate_v, up_v, down_v)):
        load_experts[i].wait()
        copy = pltpu.make_async_remote_copy(
            src_ref=ref.at[0],
            dst_ref=ref.at[1],
            send_sem=pair_send.at[i],
            recv_sem=pair_recv.at[i],
            device_id=(ep, tp + 1 - 2 * core),
            device_id_type=MESH,
        )
        copy.start()
        pairs.append(copy)
    for load in late:
        load.wait()
    mine = [
        column_of(
            jnp.sum(
                jnp.where(routes_ref[...] == xor(ep, off, groups), route_weights_ref[...], 0.0),
                axis=0,
                keepdims=True,
            )
        )
        for off in range(groups)
    ]
    arrived(shares.at[pl.ds(1, lanes - 1)], share_recv)
    mixed = shares[0].astype(F32)
    for other in range(1, lanes):
        mixed = mixed + shares[other].astype(F32)
    resid = (xf + mixed * rms_scale(mixed) * gain_out_ref[...]).astype(BF16)
    rf = resid.astype(F32)
    ffn_in = (rf * rms_scale(rf) * ffn_gain_ref[...]).astype(BF16)
    rows[...] = ffn_in

    @pl.when(core == 1)
    def _():
        pl.semaphore_wait(barrier, groups - 1)
        for off in range(groups - 1, 0, -1):
            group = xor(ep, off, groups)
            pltpu.make_async_remote_copy(
                src_ref=rows,
                dst_ref=inbox.at[slot_of(group)] if off > 1 else inbox.at[0],
                send_sem=rows_send,
                recv_sem=rows_recv.at[slot_of(group)] if off > 1 else rows_recv.at[0],
                device_id=(group, 2 * chip + off % 2),
                device_id_type=MESH,
            ).start()

    for q in range(lanes):
        resid_v[q] = rf[:, q * quarter : (q + 1) * quarter]

    @pl.when(core == 0)
    def _():
        inbox[0] = rows[...]

    @pl.when(core == 1)
    def _():
        arrived(inbox.at[0], rows_recv.at[0])

    for copy in pairs:
        copy.wait_recv()

    def result(slot, ahead, to_core):
        off = core if slot == 0 else 2 * xor(depth, depth_of(slot), slots) + core
        dst = results.at[off * chips + ahead]
        return pltpu.make_async_remote_copy(
            src_ref=parts.at[slot, lane_at(ahead, to_core)],
            dst_ref=dst,
            send_sem=parts_send.at[min(slot, 1)],
            recv_sem=parts_recv.at[0],
            device_id=(xor(ep, off, groups), lane_at(ahead, to_core)),
            device_id_type=MESH,
        )

    for slot in range(slots):
        if slot:
            arrived(inbox.at[slot], rows_recv.at[slot])
        x = inbox[slot]
        act = [
            (
                jax.nn.silu(jnp.dot(x, gate_v[block], preferred_element_type=F32))
                * jnp.dot(x, up_v[block], preferred_element_type=F32)
            ).astype(BF16)
            for block in range(2)
        ]
        for q in range(lanes):
            parts[slot, q] = sum(
                jnp.dot(
                    act[block],
                    down_v[block, :, q * quarter : (q + 1) * quarter],
                    preferred_element_type=F32,
                )
                for block in range(2)
            ).astype(BF16)
        for ahead in range(chips - 1, 0, -1):
            for to_core in range(2):
                result(slot, ahead, to_core).start()
        if slot:
            for to_core in range(2):
                result(slot, 0, to_core).start()
        else:

            @pl.when(core == 1)
            def _():
                for to_core in range(2):
                    result(0, 0, to_core).start()

            @pl.when(core == 0)
            def _():
                pltpu.make_async_remote_copy(
                    src_ref=parts.at[0, tp + 1],
                    dst_ref=results.at[0],
                    send_sem=parts_send.at[0],
                    recv_sem=parts_recv.at[1],
                    device_id=(ep, tp + 1),
                    device_id_type=MESH,
                ).start()
                results[0] = parts[0, tp]

    arrived(results.at[pl.ds(1, groups * chips - 1)], parts_recv.at[0])

    @pl.when(core == 1)
    def _():
        arrived(results.at[0], parts_recv.at[1])

    routed = None
    for off in range(groups):
        total = None
        for ahead in range(chips):
            part = results[off * chips + ahead].astype(F32)
            total = part if total is None else total + part
        term = mine[off] * total.astype(BF16).astype(F32)
        routed = term if routed is None else routed + term
    wide = squares.shape[2]
    eye = lax.broadcasted_iota(jnp.int32, (seqs, wide), 0) == lax.broadcasted_iota(
        jnp.int32, (seqs, wide), 1
    )
    squares[0] = jnp.sum(
        jnp.where(eye, jnp.sum(routed * routed, axis=1, keepdims=True), 0.0),
        axis=0,
        keepdims=True,
    )
    for ahead in range(chips - 1, -1, -1):
        for flip in range(2):
            if ahead or flip:
                pltpu.make_async_remote_copy(
                    src_ref=squares.at[0],
                    dst_ref=squares.at[2 * ahead + flip],
                    send_sem=squares_send,
                    recv_sem=squares_recv,
                    device_id=(ep, lane_at(ahead, lax.rem(core + flip, 2))),
                    device_id_type=MESH,
                ).start()
    arrived(shares.at[pl.ds(1, lanes - 1)], share_send)
    for copy in pairs:
        copy.wait_send()
    arrived(parts.at[pl.ds(1, slots - 1)], parts_send.at[1])

    @pl.when(core == 0)
    def _():
        arrived(parts.at[0, pl.ds(1, lanes - 1)], parts_send.at[0])

    @pl.when(core == 1)
    def _():
        arrived(parts.at[0], parts_send.at[0])
        hidden = gate_v.shape[2]
        arrived(gate_v.at[0, pl.ds(0, (groups - 1) * seqs * width // hidden)], rows_send)

    arrived(squares.at[pl.ds(1, lanes - 1)], squares_recv)
    total = squares[0]
    for other in range(1, lanes):
        total = total + squares[other]
    scale = jnp.sum(
        jnp.where(eye, lax.rsqrt(total / width + EPS), 0.0), axis=1, keepdims=True
    )
    scaled = routed * scale
    out_ref[...] = (resid_v[tp] + scaled * ffn_gain_out_ref[...]).astype(BF16)
    arrived(squares.at[pl.ds(1, lanes - 1)], squares_send)


def per_device(*args):
    (
        tokens,
        memory,
        log_scale,
        mix_gain_in,
        w_query,
        w_key,
        w_value,
        w_igate,
        w_fgate,
        igate_bias,
        fgate_bias,
        head_gain,
        w_output,
        mix_gain_out,
        ffn_gain_in,
        routes,
        route_weights,
        expert_gate,
        expert_up,
        expert_down,
        ffn_gain_out,
    ) = args
    groups = lax.axis_size("ep")
    lanes = lax.axis_size("tp")
    seqs, width = tokens.shape
    local_experts, _, hidden = expert_gate.shape
    top = routes.shape[1]
    if (
        local_experts != 1
        or log_scale.shape[1] != 1
        or 2 * top < groups
        or groups & (groups - 1)
        or groups < 4
        or lanes % 2
        or lanes < 4
        or memory.shape[3] % memory.shape[2]
        or (groups - 1) * seqs > hidden
        or width % hidden
    ):
        return routed_device(*args)
    quarter = width // lanes
    key_dim, value_dim = memory.shape[2:]
    vmem = pl.BlockSpec(memory_space=pltpu.VMEM)
    hbm = pl.BlockSpec(memory_space=pl.ANY)
    dma = pltpu.SemaphoreType.DMA
    pieces = 4 if seqs % 4 == 0 else 1
    operands = (
        tokens,
        memory,
        log_scale.T,
        mix_gain_in.reshape(1, -1),
        w_query,
        w_key,
        w_value,
        w_igate.T,
        w_fgate.T,
        igate_bias.reshape(1, 1),
        fgate_bias.reshape(1, 1),
        head_gain.reshape(1, -1),
        w_output,
        mix_gain_out.reshape(1, -1),
        ffn_gain_in.reshape(1, -1),
        routes.T,
        route_weights.T,
        expert_gate,
        expert_up,
        expert_down,
        ffn_gain_out.reshape(1, -1),
    )
    held = (2, 3, 7, 8, 9, 10, 11, 13, 14, 15, 16, 20)
    return pl.pallas_call(
        functools.partial(layer_kernel, groups, lanes),
        out_shape=pltpu.VMEM((seqs, quarter), BF16),
        in_specs=[hbm for _ in operands],
        out_specs=vmem,
        scratch_shapes=[
            *[pltpu.VMEM(operands[i].shape, operands[i].dtype) for i in held],
            pltpu.VMEM((seqs, width), BF16),
            pltpu.VMEM((seqs, key_dim, value_dim), F32),
            pltpu.VMEM((width, 2 * key_dim + value_dim), BF16),
            pltpu.VMEM(w_output.shape, BF16),
            pltpu.VMEM((2, width, hidden), BF16),
            pltpu.VMEM((2, width, hidden), BF16),
            pltpu.VMEM((2, hidden, width), BF16),
            pltpu.VMEM((3 * seqs, seqs * key_dim), BF16),
            pltpu.VMEM((seqs, value_dim), F32),
            pltpu.VMEM((lanes, seqs, width), BF16),
            pltpu.VMEM((seqs, width), BF16),
            pltpu.VMEM((groups // 2, seqs, width), BF16),
            pltpu.VMEM((lanes, seqs, quarter), F32),
            pltpu.VMEM((groups // 2, lanes, seqs, quarter), BF16),
            pltpu.VMEM((groups * lanes // 2, seqs, quarter), BF16),
            pltpu.VMEM((lanes, 1, 128), F32),
            dma((4,)),
            dma((6,)),
            dma((5,)),
            dma((pieces,)),
            dma((3,)),
            dma((3,)),
            dma((3,)),
            pltpu.SemaphoreType.REGULAR,
            dma(()),
            dma(()),
            dma(()),
            dma((groups // 2,)),
            dma((2,)),
            dma((2,)),
            dma(()),
            dma(()),
        ],
        compiler_params=pltpu.CompilerParams(
            collective_id=0,
            has_side_effects=True,
            vmem_limit_bytes=59 * 1024 * 1024,
        ),
        name="layer",
    )(*operands)


def solution(mesh):
    return jax.shard_map(
        per_device,
        mesh=mesh,
        in_specs=(
            P("ep", None),
            P("ep", "tp", None, None),
            P("ep", "tp"),
            P(),
            P(None, "tp"),
            P(None, "tp"),
            P(None, "tp"),
            P(None, "tp"),
            P(None, "tp"),
            P("tp"),
            P("tp"),
            P("tp"),
            P("tp", None),
            P(),
            P(),
            P("ep", None),
            P("ep", None),
            P("ep", None, "tp"),
            P("ep", None, "tp"),
            P("ep", "tp", None),
            P("tp"),
        ),
        out_specs=P("ep", "tp"),
        check_vma=False,
    )
```

time: 26.3 us -> 22.5 us (0.86)
  Pallas kernels: 24.2 us -> 20.4 us
    pallas_call x1, Pallas kernels: 24.2 us -> 20.4 us  [per_device(): pl.pallas_call(functools.partial(layer_kernel, groups, lanes), out_shape=...]
where the time goes in v1:
time: 22.5 us; the launch traced here: 22.3 us
  Pallas kernels  20.4 us (91%)
  between operations  1.3 us (6%)
  local copies, waits for them, and re-layouts  0.6 us (3%)
    pallas_call x1, Pallas kernels, per_device(): pl.pallas_call(functools.partial(layer_kernel, groups, lanes), out_shape=...  20.4 us
    unnamed x1, local copies, waits for them, and re-layouts  0.6 us

profile of v1, /device:TPU:0, one launch (start us, length us, event | category | flops | bytes accessed | tf_op | source)
XLA Modules:
  0.0 22.3 jit_solution(9372638258494144956)
XLA Ops:
  1.3 20.4 %layer.1 = bf16[16,256]{1,0:T(8,128)(2,1)S(1)} custom-call(bf16[16,1024]{1,0:T(8,128)(2,1)} %tokens_hbm.1, f32[16,1,128,256]{3,2,1,0:T(8,128)} %memory_hbm.1, f32[1,16]{1,0:T(1,128)} %bitcast.23, f32[1,1024]{1,0:T(1,128)} %bitcast.14, bf16[1024,128]{1,0:T(8,128)(2,1)} %w_query_hbm.1, bf16[1024,128]{1,0:T(8,128)(2,1)} %w_key_hbm.1, ...), custom_call_target="tpu_custom_call" | custom-call | tf_op jit(solution)/shard_map/layer/pallas_call | solution.py:638
  21.7 0.6 %copy.23 = bf16[16,256]{1,0:T(8,128)(2,1)} copy(bf16[16,256]{1,0:T(8,128)(2,1)S(1)} %layer.1) | data formatting | bytes 16384

commit v2 on v1

v2 whole, which is shorter than its diff:
```python
import functools

import jax
import jax.numpy as jnp
from jax import lax
from jax.experimental import pallas as pl
from jax.experimental.pallas import tpu as pltpu
from jax.sharding import PartitionSpec as P

EPS = 1e-06


def rms_scale(values):
    return lax.rsqrt(jnp.mean(values * values, axis=-1, keepdims=True) + EPS)


def routed_device(
    tokens,
    memory,
    log_scale,
    mix_gain_in,
    w_query,
    w_key,
    w_value,
    w_igate,
    w_fgate,
    igate_bias,
    fgate_bias,
    head_gain,
    w_output,
    mix_gain_out,
    ffn_gain_in,
    routes,
    route_weights,
    expert_gate,
    expert_up,
    expert_down,
    ffn_gain_out,
):
    f32 = jnp.float32
    bf16 = jnp.bfloat16
    seqs, width = tokens.shape
    heads = log_scale.shape[1]
    key_dim = memory.shape[2]
    value_dim = memory.shape[3]
    xf = tokens.astype(f32)
    normed = (xf * rms_scale(xf) * mix_gain_in).astype(bf16)
    query = jnp.dot(normed, w_query, preferred_element_type=f32).reshape(
        seqs, heads, key_dim
    ) * key_dim ** (-0.5)
    keys = jnp.dot(normed, w_key, preferred_element_type=f32).reshape(seqs, heads, key_dim)
    values = jnp.dot(normed, w_value, preferred_element_type=f32).reshape(seqs, heads, value_dim)
    in_pre = jnp.dot(normed, w_igate, preferred_element_type=f32) + igate_bias
    forget_log = jax.nn.log_sigmoid(
        jnp.dot(normed, w_fgate, preferred_element_type=f32) + fgate_bias
    )
    carried = forget_log + log_scale
    new_max = jnp.maximum(carried, in_pre)
    carry_weight = jnp.exp(carried - new_max)
    fresh_weight = jnp.exp(in_pre - new_max)
    recall = jnp.einsum("shk,shkv->shv", query, memory, precision=lax.Precision.HIGHEST)
    match = jnp.sum(query * keys, axis=-1)
    read = carry_weight[..., None] * recall + (fresh_weight * match)[..., None] * values
    headout = (
        (read * rms_scale(read) * head_gain.reshape(heads, value_dim))
        .astype(bf16)
        .reshape(seqs, heads * value_dim)
    )
    partial_value = jnp.dot(headout, w_output, preferred_element_type=f32)
    mixed = lax.psum(partial_value.astype(jnp.bfloat16), "tp").astype(jnp.float32)
    resid = (xf + mixed * rms_scale(mixed) * mix_gain_out).astype(bf16)
    rf = resid.astype(f32)
    ffn_in = (rf * rms_scale(rf) * ffn_gain_in).astype(bf16)
    lanes = lax.axis_size("tp")
    quarter = width // lanes
    own = lax.axis_index("tp") * quarter
    local_experts = expert_gate.shape[0]
    experts_all = local_experts * lax.axis_size("ep")
    top = routes.shape[1]
    cap = min(seqs, max(2, 3 * seqs * top // (2 * experts_all)))
    flat = routes.reshape(-1)
    hits = (flat[:, None] == jnp.arange(experts_all, dtype=jnp.int32)[None, :]).astype(jnp.int32)
    earlier = jnp.cumsum(hits, axis=0) - hits
    slot = jnp.sum(earlier * hits, axis=1)
    place = (flat * cap + slot).reshape(seqs, top)
    picker = jnp.any(
        jnp.arange(experts_all * cap, dtype=jnp.int32)[:, None, None] == place[None, :, :], axis=2
    ).astype(bf16)
    outbound = (
        jnp.dot(picker, ffn_in, preferred_element_type=f32)
        .astype(bf16)
        .reshape(experts_all, cap, width)
    )
    arrived = lax.all_to_all(outbound, "ep", split_axis=0, concat_axis=0, tiled=True)
    items = arrived.shape[1]
    rows = arrived.reshape(-1, local_experts, items, width)
    gate = jnp.einsum("secd,edf->secf", rows, expert_gate, preferred_element_type=f32)
    up = jnp.einsum("secd,edf->secf", rows, expert_up, preferred_element_type=f32)
    act = (jax.nn.silu(gate) * up).astype(bf16)
    part = jnp.einsum("secf,efd->secd", act, expert_down, preferred_element_type=f32).reshape(
        -1, items, width
    )
    summed = lax.psum_scatter(
        part.astype(jnp.bfloat16), "tp", scatter_dimension=2, tiled=True
    ).astype(jnp.float32)
    done = summed.astype(bf16)
    returned = lax.all_to_all(done, "ep", split_axis=0, concat_axis=0, tiled=True)
    columns = returned.shape[2]
    chosen = jnp.take(returned.reshape(-1, columns), place.reshape(-1), axis=0).reshape(
        seqs, top, columns
    )
    routed = jnp.sum(route_weights[:, :, None] * chosen.astype(f32), axis=1)
    resid_part = lax.dynamic_slice_in_dim(rf, own, quarter, 1)
    total = lax.psum(jnp.sum(routed * routed, axis=1), "tp")
    scaled = routed * lax.rsqrt(total / width + EPS)[:, None]
    return (resid_part + scaled * ffn_gain_out).astype(bf16)


F32 = jnp.float32
BF16 = jnp.bfloat16
MESH = pl.DeviceIdType.MESH


def column_of(row):
    n = row.shape[1]
    eye = lax.broadcasted_iota(jnp.int32, (n, n), 0) == lax.broadcasted_iota(jnp.int32, (n, n), 1)
    return jnp.sum(jnp.where(eye, jnp.broadcast_to(row, (n, n)), 0.0), axis=1, keepdims=True)


def xor(a, b, size):
    total, bit = 0, 1
    while bit < size:
        total += bit * lax.rem(a // bit + b // bit, 2)
        bit *= 2
    return total


def arrived(ref, sem):
    pltpu.make_async_copy(ref, ref, sem).wait()


def layer_kernel(
    groups,
    lanes,
    tokens_hbm,
    memory_hbm,
    log_scale_hbm,
    gain_in_hbm,
    w_query_hbm,
    w_key_hbm,
    w_value_hbm,
    w_igate_hbm,
    w_fgate_hbm,
    igate_bias_hbm,
    fgate_bias_hbm,
    head_gain_hbm,
    w_output_hbm,
    gain_out_hbm,
    ffn_gain_hbm,
    routes_hbm,
    route_weights_hbm,
    gate_hbm,
    up_hbm,
    down_hbm,
    ffn_gain_out_hbm,
    out_ref,
    log_scale_ref,
    gain_in_ref,
    routes_ref,
    route_weights_ref,
    w_gates_v,
    biases_v,
    gains_v,
    heads_v,
    tokens_v,
    memory_v,
    w_qkv_v,
    w_output_v,
    into_v,
    down_v,
    spread_v,
    wide_v,
    recall_v,
    shares,
    rows,
    inbox,
    resid_v,
    parts,
    results,
    routed_v,
    squares,
    load_sem,
    early_sem,
    late_sem,
    expert_sem,
    pair_send,
    pair_recv,
    entered,
    share_send,
    share_recv,
    rows_send,
    rows_recv,
    resid_sem,
    parts_send,
    parts_recv,
    routed_sem,
    squares_sem,
):
    ep = lax.axis_index("ep")
    tp = lax.axis_index("tp")
    seqs, width = tokens_v.shape
    key_dim = memory_v.shape[1]
    value_dim = memory_v.shape[2]
    quarter, half = width // lanes, 2 * width // lanes
    core, chip = lax.rem(tp, 2), tp // 2
    slots, chips = groups // 2, lanes // 2
    depth, side = ep // 2, lax.rem(ep, 2)
    barrier = pltpu.get_barrier_semaphore()

    def lane_at(ahead, to_core):
        return 2 * lax.rem(chip + ahead, chips) + to_core

    load_tokens = pltpu.make_async_copy(tokens_hbm, tokens_v, load_sem.at[0])
    load_gain = pltpu.make_async_copy(gain_in_hbm, gain_in_ref, load_sem.at[1])
    load_qkv = [
        pltpu.make_async_copy(src, w_qkv_v.at[:, pl.ds(at, src.shape[1])], load_sem.at[2])
        for src, at in (
            (w_query_hbm, 0),
            (w_key_hbm, key_dim),
            (w_value_hbm, 2 * key_dim),
        )
    ]
    load_output = pltpu.make_async_copy(w_output_hbm, w_output_v, load_sem.at[3])
    load_memory = pltpu.make_async_copy(memory_hbm.at[:, 0], memory_v, load_sem.at[4])

    def loads(sems, *copies):
        return [pltpu.make_async_copy(src, dst, sems.at[i]) for src, dst, i in copies]

    early = loads(
        early_sem,
        (w_igate_hbm, w_gates_v.at[0], 0),
        (w_fgate_hbm, w_gates_v.at[1], 0),
        (log_scale_hbm, log_scale_ref, 1),
        (igate_bias_hbm, biases_v.at[0], 2),
        (fgate_bias_hbm, biases_v.at[1], 2),
    )
    late = loads(
        late_sem,
        (head_gain_hbm, heads_v.at[0], 0),
        (ffn_gain_out_hbm, heads_v.at[1], 0),
        (gain_out_hbm, gains_v.at[0], 1),
        (ffn_gain_hbm, gains_v.at[1], 1),
        (routes_hbm, routes_ref, 2),
        (route_weights_hbm, route_weights_ref, 3),
    )
    experts = loads(
        expert_sem,
        (gate_hbm.at[0], into_v.at[0, 0], 0),
        (up_hbm.at[0], into_v.at[0, 1], 0),
        (down_hbm.at[0], down_v.at[0], 1),
    )
    load_tokens.start()
    load_gain.start()
    for load in early:
        load.start()
    for load in load_qkv:
        load.start()

    def depth_of(slot):
        return slot - 1 + (slot - 1 + slots - depth) // slots

    def greet(group, lane):
        pl.semaphore_signal(barrier, inc=1, device_id=(group, lane), device_id_type=MESH)

    for slot in range(1, slots):
        greet(xor(ep, 2 * slot + core, groups), 2 * chip + 1)

    @pl.when(core == 1)
    def _():
        for ahead in range(chips):
            greet(ep, lane_at(ahead, 0))
        greet(xor(ep, 1, groups), tp)

    spread_v[...] = (
        lax.rem(lax.broadcasted_iota(jnp.int32, spread_v.shape, 0), seqs)
        == lax.broadcasted_iota(jnp.int32, spread_v.shape, 1) // key_dim
    ).astype(F32).astype(BF16)

    load_memory.start()
    load_output.start()
    for load in late:
        load.start()
    load_tokens.wait()
    load_gain.wait()
    xf = tokens_v[...].astype(F32)
    normed = (xf * rms_scale(xf) * gain_in_ref[...]).astype(BF16)
    arrived(w_gates_v, early_sem.at[0])
    arrived(log_scale_ref, early_sem.at[1])
    arrived(biases_v, early_sem.at[2])
    nf = normed.astype(F32)
    in_pre = jnp.sum(nf * w_gates_v[0].astype(F32), axis=1, keepdims=True) + biases_v[0]
    fpre = jnp.sum(nf * w_gates_v[1].astype(F32), axis=1, keepdims=True) + biases_v[1]
    forget_log = jnp.minimum(fpre, 0.0) - jnp.log1p(jnp.exp(-jnp.abs(fpre)))
    carried = forget_log + column_of(log_scale_ref[...])
    new_max = jnp.maximum(carried, in_pre)
    carry_weight = jnp.exp(carried - new_max)
    fresh_weight = jnp.exp(in_pre - new_max)
    arrived(w_qkv_v, load_sem.at[2])

    @pl.when(core == 0)
    def _():
        pl.semaphore_wait(barrier, chips)
        pl.semaphore_signal(entered, inc=1, device_id=(ep, tp + 1), device_id_type=MESH)

    qkv = jnp.dot(normed, w_qkv_v[...], preferred_element_type=F32)
    query = qkv[:, :key_dim] * key_dim ** (-0.5)
    keys = qkv[:, key_dim : 2 * key_dim]
    values = qkv[:, 2 * key_dim :]
    high = query.astype(BF16).astype(F32)
    middle = (query - high).astype(BF16).astype(F32)
    low = query - high - middle
    turned = jnp.concatenate([high, middle, low], axis=0).T.astype(BF16)
    wide_v[...] = jnp.dot(turned, spread_v[...], preferred_element_type=F32)
    match = jnp.sum(query * keys, axis=1, keepdims=True)
    fresh = (fresh_weight * match) * values
    load_memory.wait()
    load_output.wait()
    arrived(heads_v, late_sem.at[0])
    for load in experts:
        load.start()
    for s in range(seqs):
        column = wide_v[:, s * key_dim : (s + 1) * key_dim]
        for at in range(0, value_dim, key_dim):
            recall_v[s : s + 1, at : at + key_dim] = jnp.sum(
                column * memory_v[s, :, at : at + key_dim], axis=0, keepdims=True
            )
    read = carry_weight * recall_v[...] + fresh
    headout = (read * heads_v[0]).astype(BF16)
    shares[0] = (
        jnp.dot(headout, w_output_v[...], preferred_element_type=F32) * rms_scale(read)
    ).astype(BF16)

    @pl.when(core == 1)
    def _():
        pl.semaphore_wait(entered, 1)


    def share(ahead):
        pltpu.make_async_remote_copy(
            src_ref=shares.at[0],
            dst_ref=shares.at[2 * ahead + 1 - core],
            send_sem=share_send,
            recv_sem=share_recv,
            device_id=(ep, lane_at(ahead, 1)),
            device_id_type=MESH,
        ).start()

    for ahead in range(1, chips):
        share(ahead)

    @pl.when(core == 0)
    def _():
        share(0)

    pairs = []
    for i, ref in enumerate((into_v, down_v)):
        arrived(ref.at[0], expert_sem.at[i])
        copy = pltpu.make_async_remote_copy(
            src_ref=ref.at[0],
            dst_ref=ref.at[1],
            send_sem=pair_send.at[i],
            recv_sem=pair_recv.at[i],
            device_id=(ep, tp + 1 - 2 * core),
            device_id_type=MESH,
        )
        copy.start()
        pairs.append(copy)
    arrived(gains_v, late_sem.at[1])
    arrived(routes_ref, late_sem.at[2])
    arrived(route_weights_ref, late_sem.at[3])
    mine = [
        column_of(
            jnp.sum(
                jnp.where(routes_ref[...] == xor(ep, off, groups), route_weights_ref[...], 0.0),
                axis=0,
                keepdims=True,
            )
        )
        for off in range(groups)
    ]

    def send_rows(group, slot, to_core):
        pltpu.make_async_remote_copy(
            src_ref=rows,
            dst_ref=inbox.at[slot],
            send_sem=rows_send,
            recv_sem=rows_recv.at[slot],
            device_id=(group, 2 * chip + to_core),
            device_id_type=MESH,
        ).start()

    @pl.when(core == 1)
    def _():
        arrived(shares.at[pl.ds(1, lanes - 1)], share_recv)
        mixed = shares[0].astype(F32)
        for other in range(1, lanes):
            mixed = mixed + shares[other].astype(F32)
        resid = (xf + mixed * rms_scale(mixed) * gains_v[0]).astype(BF16)
        rf = resid.astype(F32)
        rows[...] = (rf * rms_scale(rf) * gains_v[1]).astype(BF16)
        pl.semaphore_wait(barrier, groups - 1)
        upper = depth // (slots // 2)
        level = upper * depth + (1 - upper) * (slots - 1 - depth)
        for i in range(slots - 1):
            step = i + (i - level + slots) // slots
            to = upper * step + (1 - upper) * (slots - 1 - step)
            slot = depth + (to - depth + slots - 1) // slots
            for to_core in (1, 0):
                send_rows(2 * to + lax.rem(side + to_core, 2), slot - to_core * (1 // slot), to_core)
        send_rows(xor(ep, 1, groups), 1, 1)
        send_rows(ep, 0, 0)
        for q in range(lanes):
            resid_v[q] = resid[:, q * quarter : (q + 1) * quarter]
        pltpu.make_async_remote_copy(
            src_ref=resid_v.at[tp - 1],
            dst_ref=resid_v.at[tp - 1],
            send_sem=resid_sem.at[0],
            recv_sem=resid_sem.at[1],
            device_id=(ep, tp - 1),
            device_id_type=MESH,
        ).start()

    for copy in pairs:
        copy.wait_recv()

    nearest = depth_of(1)

    def result(slot, ahead):
        level = depth_of(slot)
        if slot < 2:
            turn = core if slot == 0 else 1 - core
            level = turn * nearest + (1 - turn) * depth
        off = 2 * xor(depth, level, slots) + core
        return pltpu.make_async_remote_copy(
            src_ref=parts.at[slot, lax.rem(chip + ahead, chips)],
            dst_ref=results.at[off * chips + ahead],
            send_sem=parts_send,
            recv_sem=parts_recv,
            device_id=(xor(ep, off, groups), lane_at(ahead, 1)),
            device_id_type=MESH,
        )

    for slot in range(slots):
        arrived(inbox.at[slot], rows_recv.at[slot])
        x = inbox[slot]
        act = [
            (
                jax.nn.silu(jnp.dot(x, into_v[block, 0], preferred_element_type=F32))
                * jnp.dot(x, into_v[block, 1], preferred_element_type=F32)
            ).astype(BF16)
            for block in range(2)
        ]
        for y in range(chips):
            parts[slot, y] = sum(
                jnp.dot(
                    act[block],
                    down_v[block, :, y * half : (y + 1) * half],
                    preferred_element_type=F32,
                )
                for block in range(2)
            ).astype(BF16)
        for ahead in range(chips - 1, -1, -1):
            result(slot, ahead).start()

    wide = squares.shape[2]
    eye = lax.broadcasted_iota(jnp.int32, (seqs, wide), 0) == lax.broadcasted_iota(
        jnp.int32, (seqs, wide), 1
    )

    def send(ref, at, sems, lane):
        pltpu.make_async_remote_copy(
            src_ref=ref.at[0],
            dst_ref=ref.at[at],
            send_sem=sems.at[0],
            recv_sem=sems.at[1],
            device_id=(ep, lane),
            device_id_type=MESH,
        ).start()

    @pl.when(core == 1)
    def _():
        arrived(results, parts_recv)
        routed = None
        for off in range(groups):
            total = None
            for ahead in range(chips):
                part = results[off * chips + ahead].astype(F32)
                total = part if total is None else total + part
            term = mine[off] * total.astype(BF16).astype(F32)
            routed = term if routed is None else routed + term
        squares[0] = jnp.sum(
            jnp.where(eye, jnp.sum(routed * routed, axis=1, keepdims=True), 0.0),
            axis=0,
            keepdims=True,
        )
        for ahead in range(chips - 1, 0, -1):
            for to_core in range(2):
                send(squares, ahead, squares_sem, lane_at(ahead, to_core))
        send(squares, 0, squares_sem, tp - 1)
        routed_v[0] = routed[:, :quarter]
        routed_v[1] = routed[:, quarter:]
        send(routed_v, 0, routed_sem, tp - 1)

    for copy in pairs:
        copy.wait_send()
    arrived(parts, parts_send)

    @pl.when(core == 0)
    def _():
        arrived(shares.at[pl.ds(0, chips)], share_send)
        arrived(resid_v.at[0], resid_sem.at[1])
        arrived(routed_v.at[0], routed_sem.at[1])
        arrived(squares.at[pl.ds(0, chips)], squares_sem.at[1])

    @pl.when(core == 1)
    def _():
        arrived(shares.at[pl.ds(0, chips - 1)], share_send)
        arrived(resid_v.at[0], resid_sem.at[0])
        arrived(routed_v.at[0], routed_sem.at[0])
        hidden = into_v.shape[3]
        arrived(into_v.at[0, 0, pl.ds(0, groups * seqs * width // hidden)], rows_send)
        arrived(squares.at[pl.ds(1, 2 * chips - 1)], squares_sem.at[0])
        arrived(squares.at[pl.ds(1, chips - 1)], squares_sem.at[1])

    total = squares[0]
    for other in range(1, chips):
        total = total + squares[other]
    scale = jnp.sum(
        jnp.where(eye, lax.rsqrt(total / width + EPS), 0.0), axis=1, keepdims=True
    )
    out_ref[...] = (
        resid_v[tp].astype(F32) + routed_v[core] * scale * heads_v[1]
    ).astype(BF16)


def per_device(*args):
    (
        tokens,
        memory,
        log_scale,
        mix_gain_in,
        w_query,
        w_key,
        w_value,
        w_igate,
        w_fgate,
        igate_bias,
        fgate_bias,
        head_gain,
        w_output,
        mix_gain_out,
        ffn_gain_in,
        routes,
        route_weights,
        expert_gate,
        expert_up,
        expert_down,
        ffn_gain_out,
    ) = args
    groups = lax.axis_size("ep")
    lanes = lax.axis_size("tp")
    seqs, width = tokens.shape
    local_experts, _, hidden = expert_gate.shape
    top = routes.shape[1]
    if (
        local_experts != 1
        or log_scale.shape[1] != 1
        or 2 * top < groups
        or groups & (groups - 1)
        or groups < 4
        or lanes % 2
        or lanes < 4
        or memory.shape[3] % memory.shape[2]
        or memory.shape[3] * lanes != width
        or groups * seqs > hidden
        or width % hidden
    ):
        return routed_device(*args)
    quarter = width // lanes
    key_dim, value_dim = memory.shape[2:]
    vmem = pl.BlockSpec(memory_space=pltpu.VMEM)
    hbm = pl.BlockSpec(memory_space=pl.ANY)
    dma = pltpu.SemaphoreType.DMA
    operands = (
        tokens,
        memory,
        log_scale.T,
        mix_gain_in.reshape(1, -1),
        w_query,
        w_key,
        w_value,
        w_igate.T,
        w_fgate.T,
        igate_bias.reshape(1, 1),
        fgate_bias.reshape(1, 1),
        head_gain.reshape(1, -1),
        w_output,
        mix_gain_out.reshape(1, -1),
        ffn_gain_in.reshape(1, -1),
        routes.T,
        route_weights.T,
        expert_gate,
        expert_up,
        expert_down,
        ffn_gain_out.reshape(1, -1),
    )
    held = (2, 3, 15, 16)
    return pl.pallas_call(
        functools.partial(layer_kernel, groups, lanes),
        out_shape=pltpu.VMEM((seqs, quarter), BF16),
        in_specs=[hbm for _ in operands],
        out_specs=vmem,
        scratch_shapes=[
            *[pltpu.VMEM(operands[i].shape, operands[i].dtype) for i in held],
            pltpu.VMEM((2, 1, width), BF16),
            pltpu.VMEM((2, 1, 1), F32),
            pltpu.VMEM((2, 1, width), F32),
            pltpu.VMEM((2, 1, quarter), F32),
            pltpu.VMEM((seqs, width), BF16),
            pltpu.VMEM((seqs, key_dim, value_dim), F32),
            pltpu.VMEM((width, 2 * key_dim + value_dim), BF16),
            pltpu.VMEM(w_output.shape, BF16),
            pltpu.VMEM((2, 2, width, hidden), BF16),
            pltpu.VMEM((2, hidden, width), BF16),
            pltpu.VMEM((3 * seqs, seqs * key_dim), BF16),
            pltpu.VMEM((key_dim, seqs * key_dim), F32),
            pltpu.VMEM((seqs, value_dim), F32),
            pltpu.VMEM((lanes, seqs, width), BF16),
            pltpu.VMEM((seqs, width), BF16),
            pltpu.VMEM((groups // 2, seqs, width), BF16),
            pltpu.VMEM((lanes, seqs, quarter), BF16),
            pltpu.VMEM((groups // 2, lanes // 2, seqs, 2 * quarter), BF16),
            pltpu.VMEM((groups * lanes // 2, seqs, 2 * quarter), BF16),
            pltpu.VMEM((2, seqs, quarter), F32),
            pltpu.VMEM((lanes, 1, 128), F32),
            dma((5,)),
            dma((3,)),
            dma((4,)),
            dma((2,)),
            dma((2,)),
            dma((2,)),
            pltpu.SemaphoreType.REGULAR,
            dma(()),
            dma(()),
            dma(()),
            dma((groups // 2,)),
            dma((2,)),
            dma(()),
            dma(()),
            dma((2,)),
            dma((2,)),
        ],
        compiler_params=pltpu.CompilerParams(
            collective_id=0,
            has_side_effects=True,
            vmem_limit_bytes=59 * 1024 * 1024,
        ),
        name="layer",
    )(*operands)


def solution(mesh):
    return jax.shard_map(
        per_device,
        mesh=mesh,
        in_specs=(
            P("ep", None),
            P("ep", "tp", None, None),
            P("ep", "tp"),
            P(),
            P(None, "tp"),
            P(None, "tp"),
            P(None, "tp"),
            P(None, "tp"),
            P(None, "tp"),
            P("tp"),
            P("tp"),
            P("tp"),
            P("tp", None),
            P(),
            P(),
            P("ep", None),
            P("ep", None),
            P("ep", None, "tp"),
            P("ep", None, "tp"),
            P("ep", "tp", None),
            P("tp"),
        ),
        out_specs=P("ep", "tp"),
        check_vma=False,
    )
```

time: 22.5 us -> 21 us (0.933)
  Pallas kernels: 20.4 us -> 18.9 us
    pallas_call x1, Pallas kernels: 20.4 us -> 18.9 us  [per_device(): pl.pallas_call(functools.partial(layer_kernel, groups, lanes), out_shape=...]
where the time goes in v2:
time: 21 us; the launch traced here: 20.8 us
  Pallas kernels  18.9 us (90%)
  between operations  1.3 us (6%)
  local copies, waits for them, and re-layouts  0.6 us (3%)
    pallas_call x1, Pallas kernels, per_device(): pl.pallas_call(functools.partial(layer_kernel, groups, lanes), out_shape=...  18.9 us
    unnamed x1, local copies, waits for them, and re-layouts  0.6 us

profile of v2, /device:TPU:0, one launch (start us, length us, event | category | flops | bytes accessed | tf_op | source)
XLA Modules:
  0.0 20.8 jit_solution(10386227206482049610)
XLA Ops:
  1.3 18.9 %layer.1 = bf16[16,256]{1,0:T(8,128)(2,1)S(1)} custom-call(bf16[16,1024]{1,0:T(8,128)(2,1)} %tokens_hbm.1, f32[16,1,128,256]{3,2,1,0:T(8,128)} %memory_hbm.1, f32[1,16]{1,0:T(1,128)} %bitcast.23, f32[1,1024]{1,0:T(1,128)} %bitcast.14, bf16[1024,128]{1,0:T(8,128)(2,1)} %w_query_hbm.1, bf16[1024,128]{1,0:T(8,128)(2,1)} %w_key_hbm.1, ...), custom_call_target="tpu_custom_call" | custom-call | tf_op jit(solution)/shard_map/layer/pallas_call | solution.py:618
  20.2 0.6 %copy.23 = bf16[16,256]{1,0:T(8,128)(2,1)} copy(bf16[16,256]{1,0:T(8,128)(2,1)S(1)} %layer.1) | data formatting | bytes 16384
